TPU v7x, 32 devices: a whole 2x2x4 slice. The times are simulated.
32 devices in a mesh: sp: 16 (over z, y, x), tp: 2 (over core).
Axes of the slice: x: 2, y: 2, z: 4, core: 2. Of those that a mesh axis runs over, the one named last changes fastest.
Arguments:
- queries: bfloat16 [4096, 512], P('sp', 'tp'), may hold values from -6 to 6
- keys: bfloat16 [4096, 512], P('sp', 'tp'), may hold values from -6 to 6
- values: bfloat16 [4096, 512], P('sp', 'tp'), may hold values from -6 to 6
- gains: float32 [2, 128], replicated, may hold values from 0.1 to 1.9
- bias_table: float32 [192, 4], P(None, 'tp'), may hold values from -6 to 270
- d_out: bfloat16 [4096, 512], P('sp', 'tp'), may hold values from -32 to 32
Outputs:
- d_queries: bfloat16 [4096, 512], P('sp', 'tp')
- d_keys: bfloat16 [4096, 512], P('sp', 'tp')
- d_values: bfloat16 [4096, 512], P('sp', 'tp')
- d_table: float32 [192, 4], P(None, 'tp')
- d_gains: float32 [2, 128], replicated
All inputs are finite; a program needn't handle non-finite values.
Results may differ from a plain program's by a relative error of at most 0.008.
Values may be sent and summed in bfloat16 or wider, within the bound.
A program may use at most 64 MiB of HBM per device.

v0:
```python
import jax
import jax.numpy as jnp
from jax import lax
from jax.sharding import PartitionSpec as P

HEADS = 4
HEAD_DIM = 128
SEG = 64
LEFT = 4
MAX_REL = 128


EPSILON = 1e-06


def shifted(block, axis, distance):
    devices = range(lax.axis_size(axis))
    route = [(i - distance, i) for i in devices if i - distance in devices]
    return lax.ppermute(block, axis, route)


def norm_rows(row_block, gain_vec):
    row_count = row_block.shape[0]
    widened = row_block.astype(jnp.float32).reshape(row_count, -1, HEAD_DIM)
    inv_rms = lax.rsqrt(jnp.mean(widened * widened, axis=-1, keepdims=True) + EPSILON)
    unit_part = widened * inv_rms
    return ((unit_part * gain_vec).astype(jnp.bfloat16).reshape(row_count, -1), unit_part, inv_rms)


def norm_back(d_normed, unit_part, inv_rms, gain_vec):
    d_unit = d_normed * gain_vec
    d_rows = inv_rms * (d_unit - unit_part * jnp.mean(d_unit * unit_part, axis=-1, keepdims=True))
    return (
        d_rows.reshape(unit_part.shape[0], -1).astype(jnp.bfloat16),
        jnp.sum(d_normed * unit_part, axis=(0, 1)),
    )


def build_bias(table_heads):
    head_count, entries = table_heads.shape
    last_entry = table_heads[:, entries - 1 :]
    padded = jnp.concatenate(
        [table_heads, jnp.broadcast_to(last_entry, (head_count, SEG - 1))], axis=1
    )
    length = entries + SEG - 1
    repeated = jnp.tile(padded, (1, SEG + 1))[:, : SEG * (length + 1)]
    hankel = repeated.reshape(head_count, SEG, length + 1)[:, :, :entries]
    near_part = hankel[:, :, ::-1]
    far_part = jnp.broadcast_to(last_entry[:, :, None], (head_count, SEG, LEFT * SEG - MAX_REL))
    return jnp.concatenate([far_part, near_part], axis=2)


def table_grad(d_band):
    head_count = d_band.shape[0]
    far_width = LEFT * SEG - MAX_REL
    far_total = jnp.sum(d_band[:, :, :far_width], axis=(1, 2))
    flipped = d_band[:, :, far_width:][:, :, ::-1]
    entries = flipped.shape[2]
    width = entries + SEG
    padded = jnp.pad(flipped, ((0, 0), (0, 0), (0, SEG)))
    skewed = padded.reshape(head_count, SEG * width)[:, : SEG * (width - 1)].reshape(
        head_count, SEG, width - 1
    )
    columns = jnp.sum(skewed, axis=1)
    tail_sum = jnp.sum(columns[:, entries - 1 :], axis=1) + far_total
    return jnp.concatenate([columns[:, : entries - 1], tail_sum[:, None]], axis=1).T


def band_of(rows_ext, seg_count):
    feature_count = rows_ext.shape[1]
    segments = rows_ext.reshape(LEFT + seg_count, SEG, feature_count)
    stacked = jnp.stack(
        [segments[offset : offset + seg_count] for offset in range(LEFT + 1)], axis=1
    )
    return stacked.reshape(seg_count, (LEFT + 1) * SEG, feature_count)


def unband(grad_band, seg_count):
    pieces = grad_band.reshape(seg_count, LEFT + 1, SEG, -1)
    summed = jnp.zeros((LEFT + seg_count, SEG, pieces.shape[3]), jnp.float32)
    for offset in range(LEFT + 1):
        summed = summed + jnp.pad(pieces[:, offset], ((offset, LEFT - offset), (0, 0), (0, 0)))
    return summed.reshape((LEFT + seg_count) * SEG, -1)


def band_grads(q_norm, d_out, k_ext, v_ext, bias_tiles, key_valid):
    seg_count = q_norm.shape[0] // SEG
    head_count = bias_tiles.shape[0]
    factor = HEAD_DIM ** (-0.5)
    q_seg = q_norm.reshape(seg_count, SEG, head_count, HEAD_DIM)
    do_seg = d_out.reshape(seg_count, SEG, head_count, HEAD_DIM)
    k_band = band_of(k_ext, seg_count).reshape(seg_count, -1, head_count, HEAD_DIM)
    v_band = band_of(v_ext, seg_count).reshape(seg_count, -1, head_count, HEAD_DIM)
    scores = (
        jnp.einsum("cihd,cjhd->chij", q_seg, k_band, preferred_element_type=jnp.float32) * factor
        + bias_tiles[None]
    )
    scores = jnp.where(key_valid, scores, -jnp.inf)
    row_max = jnp.max(scores, axis=-1, keepdims=True)
    log_total = row_max + jnp.log(jnp.sum(jnp.exp(scores - row_max), axis=-1, keepdims=True))
    prob = jnp.exp(scores - log_total)
    d_prob = jnp.einsum("cihd,cjhd->chij", do_seg, v_band, preferred_element_type=jnp.float32)
    row_delta = jnp.sum(prob * d_prob, axis=-1, keepdims=True)
    d_score = prob * (d_prob - row_delta)
    prob_low = prob.astype(jnp.bfloat16)
    d_low = d_score.astype(jnp.bfloat16)
    grad_v = jnp.einsum("chij,cihd->cjhd", prob_low, do_seg, preferred_element_type=jnp.float32)
    grad_k = (
        jnp.einsum("chij,cihd->cjhd", d_low, q_seg, preferred_element_type=jnp.float32) * factor
    )
    grad_q = (
        jnp.einsum("chij,cjhd->cihd", d_low, k_band, preferred_element_type=jnp.float32) * factor
    )
    grad_q = grad_q.reshape(seg_count * SEG, head_count, HEAD_DIM)
    return (
        grad_q,
        unband(grad_k, seg_count),
        unband(grad_v, seg_count),
        jnp.sum(d_score, axis=0),
        log_total,
        row_delta,
    )


def local(queries, keys, values, gains, bias_table, d_out):
    row_count, feature_count = queries.shape
    head_count = feature_count // HEAD_DIM
    tail_rows = LEFT * SEG
    seg_count = row_count // SEG
    device_slot = lax.axis_index("sp")
    q_norm, q_unit, q_rms = norm_rows(queries, gains[0])
    k_norm, k_unit, k_rms = norm_rows(keys, gains[1])
    earlier_k, earlier_v = shifted((k_norm, values), "sp", 1)
    k_ext = jnp.concatenate([earlier_k, k_norm])
    v_ext = jnp.concatenate([earlier_v, values])
    bias_tiles = build_bias(bias_table.T)
    band_seg = jnp.arange((LEFT + 1) * SEG, dtype=jnp.int32) // SEG
    key_seg = (
        device_slot * seg_count
        + jnp.arange(seg_count, dtype=jnp.int32)[:, None]
        - LEFT
        + band_seg[None, :]
    )
    key_valid = (key_seg >= 0)[:, None, None, :]
    d_qn, dk_ext, dv_ext, d_band, log_total, row_delta = band_grads(
        q_norm, d_out, k_ext, v_ext, bias_tiles, key_valid
    )
    dk_own = dk_ext[tail_rows:]
    dv_own = dv_ext[tail_rows:]
    back_k, back_v = (
        shifted(dk_ext[:tail_rows].astype(jnp.bfloat16), "sp", -1).astype(jnp.float32),
        shifted(dv_ext[:tail_rows].astype(jnp.bfloat16), "sp", -1).astype(jnp.float32),
    )
    dk_total = dk_own + back_k
    dv_total = dv_own + back_v
    d_queries, gain_q = norm_back(d_qn, q_unit, q_rms, gains[0])
    d_keys, gain_k = norm_back(
        dk_total.reshape(row_count, head_count, HEAD_DIM), k_unit, k_rms, gains[1]
    )
    d_values = dv_total.astype(jnp.bfloat16)
    table_part = table_grad(d_band)
    gain_part = jnp.stack([gain_q, gain_k])
    head_start = lax.axis_index("tp") * head_count
    whole_table = jnp.zeros((table_part.shape[0], HEADS), jnp.float32)
    whole_table = lax.dynamic_update_slice(whole_table, table_part, (0, head_start))
    whole_table, d_gains = lax.psum((whole_table, gain_part), ("sp", "tp"))
    d_table = lax.dynamic_slice(whole_table, (0, head_start), (table_part.shape[0], head_count))
    return (d_queries, d_keys, d_values, d_table, d_gains)


def solution(mesh):
    in_specs = (P("sp", "tp"), P("sp", "tp"), P("sp", "tp"), P(), P(None, "tp"), P("sp", "tp"))
    out_specs = (P("sp", "tp"), P("sp", "tp"), P("sp", "tp"), P(None, "tp"), P())
    return jax.shard_map(local, mesh=mesh, in_specs=in_specs, out_specs=out_specs, check_vma=False)
```

profile of v0, /device:TPU:0, one launch (start us, length us, event | category | flops | bytes accessed | tf_op | source)
XLA Modules:
  0.0 89.2 jit_solution(15028463955493800974)
XLA Ops:
  0.7 5.0 %collective-permute-start.1 = (bf16[256,256]{1,0:T(8,128)(2,1)}, bf16[256,256]{1,0:T(8,128)(2,1)S(1)}, u32[]{:S(2)}, u32[]{:S(2)}) collective-permute-start(bf16[256,256]{1,0:T(8,128)(2,1)} %param.8), channel_id=1, source_target_pairs={{0,2},{2,4},{4,6},{6,8},{8,10},{10,12},{12,14},{14,16},{16,18},{18... | collective-permute-start | bytes 393224 | tf_op jit(solution)/shard_map/ppermute | solution.py:19
  5.7 0.8 slice_bitcast_fusion.10
  6.5 1.0 %reshape.206 = f32[256,2,128]{2,1,0:T(2,128)S(1)} reshape(bf16[256,256]{1,0:T(8,128)(2,1)} %param.7) | data formatting | bytes 393216 | tf_op jit(solution)/shard_map/reshape | solution.py:24
  7.5 0.3 multiply_reduce_fusion.4
  8.3 3.4 %collective-permute-start = (bf16[256,256]{1,0:T(8,128)(2,1)S(1)}, bf16[256,256]{1,0:T(8,128)(2,1)S(1)}, u32[]{:S(2)}, u32[]{:S(2)}) collective-permute-start(bf16[256,256]{1,0:T(8,128)(2,1)S(1)} %multiply_convert_fusion.1), channel_id=1, source_target_pairs={{0,2},{2,4},{4,6},{6,8},{8,10},{10,12},{12,14},{14,16},{16,18},{18... | collective-permute-start | bytes 393224 | tf_op jit(solution)/shard_map/ppermute | solution.py:19
  11.7 0.5 broadcast_multiply_fusion.1
  12.4 0.6 broadcast_bitcast_fusion
  13.2 0.3 reduce_sum.115
  15.6 0.5 fusion.29
  16.4 0.4 multiply_reduce_fusion
  17.1 0.6 slice_reduce_fusion
  17.7 0.7 slice.172
  18.4 0.6 convolution_bitcast_fusion
  19.0 0.5 fusion
  19.6 1.5 %multiply_reduce_fusion.2 = (f32[128]{0:T(128)}, f32[4,64,2]{1,2,0:T(2,128)S(1)}, f32[4,2,128,64]{2,3,1,0:T(8,128)}) fusion(f32[4,64,2,128]{3,2,1,0:T(2,128)S(1)} %copy-done.1, f32[4,64,2]{1,2,0:T(2,128)S(1)} %copy.149, f32[128]{0:T(128)S(1)} %copy-done.23, bf16[4,2,64,320]{3,2,1,0:T(8,128)(2,1)S(1)} %get-tuple-element.12, ...), kind=kOutput, calls=%fused_computation.53 | convolution fusion | flops 42401152 | bytes 1512448 | tf_op jit(solution)/shard_map/chij,cjhd->cihd/dot_general | solution.py:112
  21.1 1.0 %reverse.1 = f32[2,64,256]{2,1,0:T(8,128)S(1)} reverse(f32[2,64,256]{2,1,0:T(8,128)} %bitcast.190), dimensions={2} | reverse | bytes 262144
  22.6 0.8 slice_reduce_fusion.1
  23.6 0.9 %copy.160 = f32[4,64,2,128]{3,2,1,0:T(2,128)} copy(f32[4,64,2,128]{3,1,2,0:T(8,128)S(1)} %multiply_bitcast_fusion) | data formatting | bytes 524288 | tf_op jit(solution)/shard_map/mul | solution.py:112
  24.5 2.1 %copy.171 = f32[4,320,2,128]{3,2,1,0:T(2,128)} copy(f32[4,320,2,128]{3,1,2,0:T(8,128)S(1)} %convolution_bitcast_fusion) | data formatting | bytes 2621440 | tf_op jit(solution)/shard_map/chij,cihd->cjhd/transpose | solution.py:107
  26.5 2.3 %reshape.213 = f32[4,5,64,256]{3,2,1,0:T(8,128)S(1)} reshape(f32[4,320,2,128]{3,2,1,0:T(2,128)} %copy.171) | data formatting | bytes 2621440 | tf_op jit(solution)/shard_map/reshape | solution.py:79
  29.1 0.7 slice.210
  29.8 1.3 %collective-permute-start.3 = (bf16[256,256]{1,0:T(8,128)(2,1)}, bf16[256,256]{1,0:T(8,128)(2,1)}, u32[]{:S(2)}, u32[]{:S(2)}) collective-permute-start(bf16[256,256]{1,0:T(8,128)(2,1)} %bitcast.44), channel_id=1, source_target_pairs={{2,0},{4,2},{6,4},{8,6},{10,8},{12,10},{14,12},{16,14},{18,16},{20... | collective-permute-start | bytes 393224 | tf_op jit(solution)/shard_map/ppermute | solution.py:19
  31.1 1.0 %copy.163 = f32[4,320,2,128]{3,2,1,0:T(2,128)S(1)} copy(f32[4,320,2,128]{3,1,2,0:T(8,128)S(1)} %fusion) | data formatting | bytes 2621440 | tf_op jit(solution)/shard_map/mul | solution.py:109
  32.1 1.0 %reshape.211 = f32[4,5,64,256]{3,2,1,0:T(8,128)S(1)} reshape(f32[4,320,2,128]{3,2,1,0:T(2,128)S(1)} %copy.163) | data formatting | bytes 2621440 | tf_op jit(solution)/shard_map/reshape | solution.py:79
  33.5 1.6 %collective-permute-start.2 = (bf16[256,256]{1,0:T(8,128)(2,1)S(1)}, bf16[256,256]{1,0:T(8,128)(2,1)S(1)}, u32[]{:S(2)}, u32[]{:S(2)}) collective-permute-start(bf16[256,256]{1,0:T(8,128)(2,1)S(1)} %bitcast.197), channel_id=1, source_target_pairs={{2,0},{4,2},{6,4},{8,6},{10,8},{12,10},{14,12},{16,14},{18,16},{20... | collective-permute-start | bytes 393224 | tf_op jit(solution)/shard_map/ppermute | solution.py:19
  35.8 0.7 fusion.15
  36.8 4.3 %collective-permute-done.2 = bf16[256,256]{1,0:T(8,128)(2,1)S(1)} collective-permute-done((bf16[256,256]{1,0:T(8,128)(2,1)S(1)}, bf16[256,256]{1,0:T(8,128)(2,1)S(1)}, u32[]{:S(2)}, u32[]{:S(2)}) %collective-permute-start.2) | collective-permute-done | bytes 131104 | tf_op jit(solution)/shard_map/ppermute | solution.py:19
  41.4 0.6 multiply_reduce_fusion.3
  42.4 0.7 fusion.12
  43.1 43.9 %all-reduce.11 = (f32[192,4]{0,1:T(4,128)S(1)}, f32[2,128]{1,0:T(2,128)}) all-reduce(f32[192,4]{0,1:T(4,128)S(1)} %fusion.26, f32[2,128]{1,0:T(2,128)S(1)} %pad_maximum_fusion.3), channel_id=1, replica_groups=mesh['sp'=16,'tp'=2] {'sp','tp'}, use_global_device_ids=true, to_apply=%region_11.12 | all-reduce | flops 1024 | bytes 8192 | tf_op jit(solution)/shard_map/psum | solution.py:166
  87.0 0.6 constant_dynamic-slice_fusion
  87.6 1.6 %fusion.16 = bf16[256,256]{1,0:T(8,128)(2,1)} fusion(f32[4,64,256]{2,1,0:T(8,128)S(1)} %slice-done, bf16[256,256]{1,0:T(8,128)(2,1)} %collective-permute-done.3), kind=kLoop, calls=%fused_computation.47 | loop fusion | flops 196608 | bytes 524288 | tf_op jit(solution)/shard_map/convert_element_type | solution.py:160
  (122 shorter events, 5.8 us)
Async XLA Ops:
  0.6 11.1 %copy-start.19 = (f32[2,128]{1,0:T(2,128)S(1)}, f32[2,128]{1,0:T(2,128)}, u32[]{:S(2)}) copy-start(f32[2,128]{1,0:T(2,128)} %param.9) | copy-start | bytes 3076
  0.6 7.6 %copy-start.4 = (bf16[256,256]{1,0:T(8,128)(2,1)S(1)}, bf16[256,256]{1,0:T(8,128)(2,1)}, u32[]{:S(2)}) copy-start(bf16[256,256]{1,0:T(8,128)(2,1)} %param.7) | copy-start | bytes 393220
  0.7 11.6 %copy-start.17 = (f32[192,2]{0,1:T(2,128)S(1)}, f32[192,2]{0,1:T(2,128)}, u32[]{:S(2)}) copy-start(f32[192,2]{0,1:T(2,128)} %param.10) | copy-start | bytes 4612
  0.7 12.3 %copy-start.7 = (bf16[256,256]{1,0:T(8,128)(2,1)S(1)}, bf16[256,256]{1,0:T(8,128)(2,1)}, u32[]{:S(2)}) copy-start(bf16[256,256]{1,0:T(8,128)(2,1)} %param.6) | copy-start | bytes 393220
  0.7 14.2 %collective-permute-start.1 = (bf16[256,256]{1,0:T(8,128)(2,1)}, bf16[256,256]{1,0:T(8,128)(2,1)S(1)}, u32[]{:S(2)}, u32[]{:S(2)}) collective-permute-start(bf16[256,256]{1,0:T(8,128)(2,1)} %param.8), channel_id=1, source_target_pairs={{0,2},{2,4},{4,6},{6,8},{8,10},{10,12},{12,14},{14,16},{16,18},{18... | collective-permute-start | bytes 393224 | tf_op jit(solution)/shard_map/ppermute | solution.py:19
  7.5 6.0 %copy-start.2 = (f32[256,2,128]{2,1,0:T(2,128)}, f32[256,2,128]{2,1,0:T(2,128)S(1)}, u32[]{:S(2)}) copy-start(f32[256,2,128]{2,1,0:T(2,128)S(1)} %reshape.206) | copy-start | bytes 786436
  7.9 6.0 %copy-start.11 = (f32[256,2]{1,0:T(8,128)}, f32[256,2]{1,0:T(8,128)S(1)}, u32[]{:S(2)}) copy-start(f32[256,2]{1,0:T(8,128)S(1)} %add_rsqrt_fusion) | copy-start | bytes 6148
  8.2 5.7 %copy-start.16 = (bf16[256,256]{1,0:T(8,128)(2,1)S(1)}, bf16[256,256]{1,0:T(8,128)(2,1)}, u32[]{:S(2)}) copy-start(bf16[256,256]{1,0:T(8,128)(2,1)} %param.11) | copy-start | bytes 393220
  8.3 6.7 %collective-permute-start = (bf16[256,256]{1,0:T(8,128)(2,1)S(1)}, bf16[256,256]{1,0:T(8,128)(2,1)S(1)}, u32[]{:S(2)}, u32[]{:S(2)}) collective-permute-start(bf16[256,256]{1,0:T(8,128)(2,1)S(1)} %multiply_convert_fusion.1), channel_id=1, source_target_pairs={{0,2},{2,4},{4,6},{6,8},{8,10},{10,12},{12,14},{14,16},{16,18},{18... | collective-permute-start | bytes 393224 | tf_op jit(solution)/shard_map/ppermute | solution.py:19
  13.6 1.3 %copy-start.9 = (f32[256,2]{1,0:T(8,128)}, f32[256,2]{1,0:T(8,128)S(1)}, u32[]{:S(2)}) copy-start(f32[256,2]{1,0:T(8,128)S(1)} %add_rsqrt_fusion.1) | copy-start | bytes 6148
  13.9 1.6 %copy-start = (f32[4,64,2,128]{3,2,1,0:T(2,128)}, f32[4,64,2,128]{3,2,1,0:T(2,128)S(1)}, u32[]{:S(2)}) copy-start(f32[4,64,2,128]{3,2,1,0:T(2,128)S(1)} %reshape.207) | copy-start | bytes 786436
  13.9 1.0 %copy-start.14 = (bf16[256,256]{1,0:T(8,128)(2,1)S(1)}, bf16[256,256]{1,0:T(8,128)(2,1)}, u32[]{:S(2)}) copy-start(bf16[256,256]{1,0:T(8,128)(2,1)} %param.8) | copy-start | bytes 393220
  17.1 1.9 %copy-start.1 = (f32[4,64,2,128]{3,2,1,0:T(2,128)S(1)}, f32[4,64,2,128]{3,2,1,0:T(2,128)}, u32[]{:S(2)}) copy-start(f32[4,64,2,128]{3,2,1,0:T(2,128)} %copy-done) | copy-start | bytes 786436
  19.0 0.7 copy-start.23
  21.1 2.4 %copy-start.15 = (f32[4,2,128,64]{2,3,1,0:T(8,128)S(1)}, f32[4,2,128,64]{2,3,1,0:T(8,128)}, u32[]{:S(2)}) copy-start(f32[4,2,128,64]{2,3,1,0:T(8,128)} %get-tuple-element.35) | copy-start | bytes 786436
  29.1 7.5 %copy-start.6 = (f32[8,64,256]{2,1,0:T(8,128)}, f32[8,64,256]{2,1,0:T(8,128)S(1)}, u32[]{:S(2)}) copy-start(f32[8,64,256]{2,1,0:T(8,128)S(1)} %pad_add_fusion) | copy-start | bytes 1572868
  29.8 57.8 %collective-permute-start.3 = (bf16[256,256]{1,0:T(8,128)(2,1)}, bf16[256,256]{1,0:T(8,128)(2,1)}, u32[]{:S(2)}, u32[]{:S(2)}) collective-permute-start(bf16[256,256]{1,0:T(8,128)(2,1)} %bitcast.44), channel_id=1, source_target_pairs={{2,0},{4,2},{6,4},{8,6},{10,8},{12,10},{14,12},{16,14},{18,16},{20... | collective-permute-start | bytes 393224 | tf_op jit(solution)/shard_map/ppermute | solution.py:19
  33.3 1.8 %copy-start.10 = (f32[256,2]{1,0:T(8,128)S(1)}, f32[256,2]{1,0:T(8,128)}, u32[]{:S(2)}) copy-start(f32[256,2]{1,0:T(8,128)} %copy-done.9) | copy-start | bytes 6148
  33.3 2.5 %copy-start.8 = (bf16[256,256]{1,0:T(8,128)(2,1)S(1)}, bf16[256,256]{1,0:T(8,128)(2,1)}, u32[]{:S(2)}) copy-start(bf16[256,256]{1,0:T(8,128)(2,1)} %param.6) | copy-start | bytes 393220
  33.3 2.5 %copy-start.13 = (f32[4,64,2,128]{3,2,1,0:T(2,128)S(1)}, f32[4,64,2,128]{3,2,1,0:T(2,128)}, u32[]{:S(2)}) copy-start(f32[4,64,2,128]{3,2,1,0:T(2,128)} %copy.160) | copy-start | bytes 786436
  33.3 2.5 %copy-start.18 = (f32[256]{0:T(256)S(1)}, f32[256]{0:T(256)}, u32[]{:S(2)}) copy-start(f32[256]{0:T(256)} %broadcast_bitcast_fusion) | copy-start | bytes 3076
  33.4 3.1 %copy-start.20 = (f32[2]{0:T(128)S(1)}, f32[2]{0:T(128)}, u32[]{:S(2)}) copy-start(f32[2]{0:T(128)} %slice_reduce_fusion) | copy-start | bytes 28
  33.4 3.1 %copy-start.22 = (f32[2]{0:T(128)S(1)}, f32[2]{0:T(128)}, u32[]{:S(2)}) copy-start(f32[2]{0:T(128)} %slice_reduce_fusion.1) | copy-start | bytes 28
  33.5 7.6 %collective-permute-start.2 = (bf16[256,256]{1,0:T(8,128)(2,1)S(1)}, bf16[256,256]{1,0:T(8,128)(2,1)S(1)}, u32[]{:S(2)}, u32[]{:S(2)}) collective-permute-start(bf16[256,256]{1,0:T(8,128)(2,1)S(1)} %bitcast.197), channel_id=1, source_target_pairs={{2,0},{4,2},{6,4},{8,6},{10,8},{12,10},{14,12},{16,14},{18,16},{20... | collective-permute-start | bytes 393224 | tf_op jit(solution)/shard_map/ppermute | solution.py:19
  35.4 5.7 %copy-start.5 = (bf16[256,256]{1,0:T(8,128)(2,1)S(1)}, bf16[256,256]{1,0:T(8,128)(2,1)}, u32[]{:S(2)}) copy-start(bf16[256,256]{1,0:T(8,128)(2,1)} %param.7) | copy-start | bytes 393220
  36.6 4.8 %copy-start.3 = (f32[256,2,128]{2,1,0:T(2,128)S(1)}, f32[256,2,128]{2,1,0:T(2,128)}, u32[]{:S(2)}) copy-start(f32[256,2,128]{2,1,0:T(2,128)} %copy-done.2) | copy-start | bytes 786436
  36.6 4.8 %copy-start.12 = (f32[256,2]{1,0:T(8,128)S(1)}, f32[256,2]{1,0:T(8,128)}, u32[]{:S(2)}) copy-start(f32[256,2]{1,0:T(8,128)} %copy-done.11) | copy-start | bytes 6148
  41.4 1.7 %copy-start.21 = (f32[128]{0:T(128)S(1)}, f32[128]{0:T(128)}, u32[]{:S(2)}) copy-start(f32[128]{0:T(128)} %get-tuple-element.5) | copy-start | bytes 1540
  41.4 46.2 %slice-start = ((f32[8,64,256]{2,1,0:T(8,128)}), f32[4,64,256]{2,1,0:T(8,128)S(1)}, s32[]{:S(2)}) async-start(f32[8,64,256]{2,1,0:T(8,128)} %copy-done.6), calls=%async_computation | async-start | bytes 524288 | tf_op jit(solution)/shard_map/slice | solution.py:149
where the time goes:
time: 89.6 us; the launch traced here: 89.2 us
  blocking collectives  43.9 us (49%)
  local copies, waits for them, and re-layouts  17.2 us (19%)
  starting transfers between devices  11.3 us (13%)
  other arithmetic  7.59 us (8%)
  waiting for transfers between devices  4.33 us (5%)
  matrix products  3.45 us (4%)
  between operations  1.42 us (2%)
    psum x1, blocking collectives, local(): whole_table, d_gains = lax.psum((whole_table, gain_part), ('sp', 'tp'))  43.9 us
    ppermute x4, starting transfers between devices, shifted(): return lax.ppermute(block, axis, route)  11.3 us
    ppermute x4, waiting for transfers between devices, shifted(): return lax.ppermute(block, axis, route)  4.33 us
    reshape x2, local copies, waits for them, and re-layouts, unband(): pieces = grad_band.reshape(seg_count, LEFT + 1, SEG, -1)  3.38 us
    transpose x1, local copies, waits for them, and re-layouts, band_grads(): jnp.einsum('chij,cihd->cjhd', prob_low, do_seg, preferred_element_type=jn...  2.07 us
    unnamed x64, local copies, waits for them, and re-layouts  2.01 us
  transfers between devices with their start and end apart: 4, of which 1 were waited for; matrix products, arithmetic and copies ran while one was open for 13% of the time, Pallas kernels for 0%

commit v1 on v0

v1 whole, which is shorter than its diff:
```python
import functools

import jax
import jax.numpy as jnp
from jax import lax
from jax.experimental import pallas as pl
from jax.experimental.pallas import tpu as pltpu
from jax.sharding import PartitionSpec as P

HEAD_DIM = 128
SEG = 64
LEFT = 4
MAX_REL = 128
EPSILON = 1e-06
NEG = -1e30
MESH = pl.DeviceIdType.MESH
F32 = jnp.float32
BF16 = jnp.bfloat16


def dot(a, b, contract, precision=None):
    return lax.dot_general(
        a, b, ((contract[:1], contract[1:]), ((), ())), preferred_element_type=F32, precision=precision
    )


def unit_of(block):
    wide = block.astype(F32)
    rms = lax.rsqrt(jnp.mean(wide * wide, axis=-1, keepdims=True) + EPSILON)
    return wide * rms, rms


def kernel(
    n_sp, n_tp,
    q_ref, k_ref, v_ref, do_ref, g_ref, t_ref,
    dq_ref, dk_ref, dv_ref, dt_ref, dg_ref,
    k_raw, k_ext, v_ext, q_nxt, do_nxt, bias, bias_t, dk_acc, dv_acc,
    st_out, st_in, red_src, red,
    send_sem, recv_sem, red_send, red_recv,
):
    rows, width = q_ref.shape
    heads = width // HEAD_DIM
    half = rows // 2
    window = rows + half
    entries = t_ref.shape[0]
    factor = HEAD_DIM ** (-0.5)
    sp, tp = lax.axis_index("sp"), lax.axis_index("tp")
    total = n_sp * n_tp
    me = sp * n_tp + tp
    has_prev, has_next = sp > 0, sp < n_sp - 1

    def place(offset):
        other = lax.rem(me + offset, total)
        return lax.div(other, n_tp), lax.rem(other, n_tp)

    barrier = pltpu.get_barrier_semaphore()

    @pl.loop(1, total)
    def _(offset):
        pl.semaphore_signal(barrier, inc=1, device_id=place(offset), device_id_type=MESH)

    pl.semaphore_wait(barrier, total - 1)

    def part(ref, index):
        return ref.at[pl.ds(index * half, half)]

    def send(slot, src, dst, to):
        return pltpu.make_async_remote_copy(
            src_ref=src, dst_ref=dst, send_sem=send_sem.at[slot], recv_sem=recv_sem.at[slot],
            device_id=(to, tp), device_id_type=MESH,
        )

    nxt, prv = sp + 1, sp - 1
    forward = [
        send(0, part(k_ref, 1), part(k_raw, 1), nxt),
        send(1, part(v_ref, 1), part(v_ext, 1), nxt),
        send(2, part(k_ref, 0), part(k_raw, 0), nxt),
        send(3, part(v_ref, 0), part(v_ext, 0), nxt),
    ]
    back = [
        send(4, part(q_ref, 0), part(q_nxt, 0), prv),
        send(5, part(do_ref, 0), part(do_nxt, 0), prv),
        send(6, part(q_ref, 1), part(q_nxt, 1), prv),
        send(7, part(do_ref, 1), part(do_nxt, 1), prv),
    ]
    stats = [send(8 + i, st_out.at[i], st_in.at[i], prv) for i in range(2)]

    @pl.when(has_next)
    def _():
        for copy in forward:
            copy.start()

    @pl.when(has_prev)
    def _():
        for copy in back:
            copy.start()

    @pl.when(jnp.logical_not(has_prev))
    def _():
        k_ext[0:rows, :] = jnp.zeros((rows, width), BF16)
        v_ext[0:rows, :] = jnp.zeros((rows, width), BF16)

    head = [slice(h * HEAD_DIM, (h + 1) * HEAD_DIM) for h in range(heads)]
    g0, g1 = g_ref[0:1, :], g_ref[1:2, :]

    row = lax.broadcasted_iota(jnp.int32, (half, rows), 0)
    col = lax.broadcasted_iota(jnp.int32, (half, rows), 1)
    flip = (
        lax.broadcasted_iota(jnp.int32, (entries, rows), 0)
        + lax.broadcasted_iota(jnp.int32, (entries, rows), 1)
        == entries - 1
    ).astype(F32)
    base = dot(t_ref[...], flip, (0, 0), lax.Precision.HIGHEST)
    for h in range(heads):
        far = base[h : h + 1, 0:1]
        near = pltpu.roll(
            jnp.broadcast_to(base[h : h + 1, :], (half, rows)), 0, 1, stride=1, stride_axis=0
        )
        near = jnp.where(col <= row, far, near)
        near = jnp.where((col >= rows - SEG) & (row < SEG), NEG, near)
        first = jnp.where((col < SEG) & (row >= SEG), NEG, jnp.broadcast_to(far, (half, rows)))
        bias[h, :, 0:half] = first[:, 0:half]
        bias[h, :, half:] = near
        bias_t[h, 0:half, :] = first[:, 0:half].T
        bias_t[h, half:, :] = near[:, 0:half].T

    v_ext[rows:, :] = v_ref[...]
    for h in range(heads):
        k_ext[rows:, head[h]] = (unit_of(k_ref[:, head[h]])[0] * g1).astype(BF16)

    lane = lax.broadcasted_iota(jnp.int32, (half, HEAD_DIM), 1)
    window_col = lax.broadcasted_iota(jnp.int32, (1, window), 1)
    d_band = [None] * heads
    gain_q = jnp.zeros((1, HEAD_DIM), F32)
    gain_k = jnp.zeros((1, HEAD_DIM), F32)
    for pair in (1, 0):
        @pl.when(has_prev)
        def _():
            forward[2 * (1 - pair)].wait_recv()
            for h in range(heads):
                block = k_raw[pair * half : (pair + 1) * half, head[h]]
                k_ext[pair * half : (pair + 1) * half, head[h]] = (unit_of(block)[0] * g1).astype(BF16)
            forward[2 * (1 - pair) + 1].wait_recv()

        own = slice(pair * half, (pair + 1) * half)
        span = slice(pair * half, pair * half + window)
        before = rows - pair * half
        absent = jnp.where((window_col < before) & jnp.logical_not(has_prev), NEG, 0.0)
        table = jnp.zeros((half, HEAD_DIM), F32)
        for h in range(heads):
            unit, rms = unit_of(q_ref[own, head[h]])
            q_norm = (unit * g0).astype(BF16)
            d_o = do_ref[own, head[h]]
            k_win, v_win = k_ext[span, head[h]], v_ext[span, head[h]]
            scores = dot(q_norm, k_win, (1, 1)) * factor + bias[h] + absent
            top = jnp.max(scores, axis=-1, keepdims=True)
            e = jnp.exp(scores - top)
            denom = jnp.sum(e, axis=-1, keepdims=True)
            prob = e * (1.0 / denom)
            d_prob = dot(d_o, v_win, (1, 1))
            delta = jnp.sum(prob * d_prob, axis=-1, keepdims=True)
            d_score = prob * (d_prob - delta)
            table = jnp.where(lane == 2 * h, top + jnp.log(denom), table)
            table = jnp.where(lane == 2 * h + 1, delta, table)
            prob_low, d_low = prob.astype(BF16), d_score.astype(BF16)
            d_qn = dot(d_low, k_win, (1, 0)) * factor
            d_v = dot(prob_low[:, before:], d_o, (0, 0))
            d_k = dot(d_low[:, before:], q_norm, (0, 0))
            if pair == 1:
                dk_acc[:, head[h]] = d_k
                dv_acc[:, head[h]] = d_v
                d_band[h] = d_score
            else:
                dk_acc[0:half, head[h]] += d_k
                dv_acc[0:half, head[h]] += d_v
                d_band[h] = d_band[h] + d_score
            grad = d_qn * g0
            out = rms * (grad - unit * jnp.mean(grad * unit, axis=-1, keepdims=True))
            dq_ref[own, head[h]] = out.astype(BF16)
            gain_q += jnp.sum(d_qn * unit, axis=0, keepdims=True)
            gain_k += jnp.sum(d_qn * q_norm.astype(F32), axis=0, keepdims=True)
        st_out[pair] = table.T[0:8, :]

        @pl.when(has_prev)
        def _():
            stats[pair].start()

    lines = []
    for h in range(heads):
        near = d_band[h][:, half:]
        near_part = jnp.where(col > row, near, 0.0)
        far_sum = jnp.sum(d_band[h][:, 0:half] + (near - near_part)[:, 0:half], keepdims=True)
        step = half // 2
        while step:
            near_part = near_part[0:step] + pltpu.roll(near_part[step : 2 * step], rows - step, 1)
            step //= 2
        near_part = jnp.where(col[0:1] == 0, far_sum, near_part)
        lines += [near_part[:, 0:half], near_part[:, half:]]
    lines += [gain_q, gain_k]
    lines += [jnp.zeros((8 - len(lines), HEAD_DIM), F32)]
    packed = jnp.concatenate(lines, axis=0)
    red_src[...] = packed
    slot = tp * n_sp + sp
    red[slot] = packed

    @pl.loop(1, total)
    def _(offset):
        pltpu.make_async_remote_copy(
            src_ref=red_src, dst_ref=red.at[slot], send_sem=red_send, recv_sem=red_recv,
            device_id=place(offset), device_id_type=MESH,
        ).start()

    @pl.when(has_next)
    def _():
        for pair in (0, 1):
            own = slice(pair * half, rows)
            src = slice(pair * half, (pair + 1) * half)
            count = rows - pair * half
            back[2 * pair].wait_recv()
            back[2 * pair + 1].wait_recv()
            stats[pair].wait_recv()
            for h in range(heads):
                q_norm = (unit_of(q_nxt[src, head[h]])[0] * g0).astype(BF16)
                d_o = do_nxt[src, head[h]]
                k_own = k_ext[rows + pair * half : 2 * rows, head[h]]
                v_own = v_ext[rows + pair * half : 2 * rows, head[h]]
                scores = dot(k_own, q_norm, (1, 1)) * factor + bias_t[h, 0:count, :]
                prob = jnp.exp(scores - st_in[pair, 2 * h : 2 * h + 1, :])
                d_prob = dot(v_own, d_o, (1, 1))
                d_score = prob * (d_prob - st_in[pair, 2 * h + 1 : 2 * h + 2, :])
                dv_acc[own, head[h]] += dot(prob.astype(BF16), d_o, (1, 0))
                dk_acc[own, head[h]] += dot(d_score.astype(BF16), q_norm, (1, 0))

    dv_ref[...] = dv_acc[...].astype(BF16)
    for h in range(heads):
        unit, rms = unit_of(k_ref[:, head[h]])
        grad = dk_acc[:, head[h]] * factor * g1
        out = rms * (grad - unit * jnp.mean(grad * unit, axis=-1, keepdims=True))
        dk_ref[:, head[h]] = out.astype(BF16)

    peers = red.at[pl.ds(0, total - 1)]
    pltpu.make_async_copy(peers, peers, red_recv).wait()
    everyone = jnp.sum(red[...], axis=0)
    mine = jnp.sum(red[pl.ds(tp * n_sp, n_sp)], axis=0)
    band = jnp.concatenate(
        [
            jnp.concatenate([mine[2 * h : 2 * h + 1], mine[2 * h + 1 : 2 * h + 2]], axis=1)
            for h in range(heads)
        ],
        axis=0,
    )
    dt_ref[...] = dot(flip, band, (1, 1), lax.Precision.HIGHEST)
    dg_ref[0:1, :] = everyone[2 * heads : 2 * heads + 1]
    dg_ref[1:2, :] = everyone[2 * heads + 1 : 2 * heads + 2] / g1

    pltpu.make_async_copy(peers, peers, red_send).wait()

    @pl.when(has_next)
    def _():
        for copy in forward:
            copy.wait_send()

    @pl.when(has_prev)
    def _():
        for copy in back + stats:
            copy.wait_send()


def solution(mesh):
    n_sp, n_tp = mesh.shape["sp"], mesh.shape["tp"]

    def local(queries, keys, values, gains, bias_table, d_out):
        rows, width = queries.shape
        heads = width // HEAD_DIM
        assert rows == LEFT * SEG and 2 * heads + 2 <= 8
        total = n_sp * n_tp
        act = jax.ShapeDtypeStruct((rows, width), BF16)
        half = rows // 2
        vmem = pl.BlockSpec(memory_space=pltpu.VMEM)
        return pl.pallas_call(
            functools.partial(kernel, n_sp, n_tp),
            out_shape=(
                act, act, act,
                jax.ShapeDtypeStruct(bias_table.shape, F32),
                jax.ShapeDtypeStruct(gains.shape, F32),
            ),
            in_specs=[vmem] * 6,
            out_specs=(vmem,) * 5,
            scratch_shapes=[
                pltpu.VMEM((rows, width), BF16),
                pltpu.VMEM((2 * rows, width), BF16),
                pltpu.VMEM((2 * rows, width), BF16),
                pltpu.VMEM((rows, width), BF16),
                pltpu.VMEM((rows, width), BF16),
                pltpu.VMEM((heads, half, rows + half), F32),
                pltpu.VMEM((heads, rows, half), F32),
                pltpu.VMEM((rows, width), F32),
                pltpu.VMEM((rows, width), F32),
                pltpu.VMEM((2, 8, half), F32),
                pltpu.VMEM((2, 8, half), F32),
                pltpu.VMEM((8, HEAD_DIM), F32),
                pltpu.VMEM((total, 8, HEAD_DIM), F32),
                pltpu.SemaphoreType.DMA((10,)),
                pltpu.SemaphoreType.DMA((10,)),
                pltpu.SemaphoreType.DMA,
                pltpu.SemaphoreType.DMA,
            ],
            compiler_params=pltpu.CompilerParams(collective_id=0, has_side_effects=True),
        )(queries, keys, values, d_out, gains, bias_table)

    in_specs = (P("sp", "tp"), P("sp", "tp"), P("sp", "tp"), P(), P(None, "tp"), P("sp", "tp"))
    out_specs = (P("sp", "tp"), P("sp", "tp"), P("sp", "tp"), P(None, "tp"), P())
    return jax.shard_map(local, mesh=mesh, in_specs=in_specs, out_specs=out_specs, check_vma=False)
```

time: 89.6 us -> 37.3 us (0.42)
  blocking collectives: 43.9 us -> 0 us
  Pallas kernels: 0 us -> 29.6 us
  starting transfers between devices: 11.3 us -> 0 us
  local copies, waits for them, and re-layouts: 17.2 us -> 6.78 us
  other arithmetic: 7.59 us -> 0 us
  waiting for transfers between devices: 4.33 us -> 0 us
  matrix products: 3.45 us -> 0 us
    psum x1 -> x0, blocking collectives: 43.9 us -> none  [local(): whole_table, d_gains = lax.psum((whole_table, gain_part), ('sp', 'tp'))]
    pallas_call x0 -> x1, Pallas kernels: none -> 29.6 us  [local(): pl.pallas_call(functools.partial(kernel, n_sp, n_tp), out_shape=(act, act...]
    ppermute x4 -> x0, starting transfers between devices: 11.3 us -> none  [shifted(): return lax.ppermute(block, axis, route)]
    reshape x7 -> x0, local copies, waits for them, and re-layouts: 4.92 us -> none  [the longest x2 3.38 us: unband(): pieces = grad_band.reshape(seg_count, LEFT + 1, SEG, -1)]
    mul x10 -> x0, local copies, waits for them, and re-layouts: 4.7 us -> none  [the longest x3 1.33 us: norm_rows(): unit_part * gain_vec]
    ppermute x4 -> x0, waiting for transfers between devices: 4.33 us -> none  [shifted(): return lax.ppermute(block, axis, route)]
    dot_general x5 -> x0, matrix products: 3.45 us -> none  [the longest x1 1.48 us: band_grads(): jnp.einsum('chij,cjhd->cihd', d_low, k_band, preferred_element_type=jnp.f...]
    reduce_sum x10 -> x0, other arithmetic: 3.4 us -> none  [the longest x1 0.77 us: table_grad(): tail_sum = jnp.sum(columns[:, entries - 1:], axis=1) + far_total]
  transfers between devices with their start and end apart: 4 -> 0, of which waited for: 1 -> 0; matrix products, arithmetic and copies ran while one was open for 13% -> 0% of each run, Pallas kernels for 0% -> 0%
where the time goes in v1:
time: 37.3 us; the launch traced here: 37 us
  Pallas kernels  29.6 us (79%)
  local copies, waits for them, and re-layouts  6.78 us (18%)
  between operations  0.64 us (2%)
    pallas_call x1, Pallas kernels, local(): pl.pallas_call(functools.partial(kernel, n_sp, n_tp), out_shape=(act, act...  29.6 us
    unnamed x11, local copies, waits for them, and re-layouts  5.23 us
    pallas_call x1, local copies, waits for them, and re-layouts, local(): pl.pallas_call(functools.partial(kernel, n_sp, n_tp), out_shape=(act, act...  1.55 us

profile of v1, /device:TPU:0, one launch (start us, length us, event | category | flops | bytes accessed | tf_op | source)
XLA Modules:
  0.0 37.0 jit_solution(9344062858277897835)
XLA Ops:
  0.6 1.4 %copy.11.t_ref = f32[192,2]{1,0:T(8,128)} copy(f32[192,2]{0,1:T(2,128)} %param.10) | data formatting | bytes 3072 | tf_op args[4]
  2.1 29.6 %shard_map.101 = (bf16[256,256]{1,0:T(8,128)(2,1)}, bf16[256,256]{1,0:T(8,128)(2,1)}, bf16[256,256]{1,0:T(8,128)(2,1)}, f32[192,2]{1,0:T(8,128)}, f32[2,128]{1,0:T(2,128)}) custom-call(bf16[256,256]{1,0:T(8,128)(2,1)} %q_ref.1, bf16[256,256]{1,0:T(8,128)(2,1)} %k_ref.1, bf16[256,256]{1,0:T(8,128)(2,1)} %v_ref.1, bf16[256,256]{1,0:T(8,128)(2,1)} %do_ref.1, ...), custom_call_target="tpu_custom_call" | custom-call | tf_op jit(solution)/shard_map/pallas_call | solution.py:280
  31.7 1.6 %copy.12 = f32[192,2]{0,1:T(2,128)} copy(f32[192,2]{1,0:T(8,128)} %get-tuple-element.8) | data formatting | bytes 3072 | tf_op jit(solution)/shard_map/pallas_call | solution.py:280
  33.2 0.0 copy-start.1
  33.2 1.6 %copy.17 = bf16[256,256]{1,0:T(8,128)(2,1)} copy(bf16[256,256]{1,0:T(8,128)(2,1)} %get-tuple-element.15) | data formatting | bytes 262144
  34.8 0.0 copy-done.1
  34.8 0.0 copy-start
  34.8 0.7 %copy.18 = bf16[256,256]{1,0:T(8,128)(2,1)} copy(bf16[256,256]{1,0:T(8,128)(2,1)S(1)} %copy-done.1) | data formatting | bytes 262144
  35.5 0.3 copy-done
  35.8 0.0 copy-start.2
  35.8 0.7 %copy.19 = bf16[256,256]{1,0:T(8,128)(2,1)} copy(bf16[256,256]{1,0:T(8,128)(2,1)S(1)} %copy-done) | data formatting | bytes 262144
  36.5 0.0 copy-done.2
  36.5 0.6 %copy.20 = f32[2,128]{1,0:T(2,128)} copy(f32[2,128]{1,0:T(2,128)S(1)} %copy-done.2) | data formatting | bytes 2048
Async XLA Ops:
  33.2 1.6 %copy-start.1 = (bf16[256,256]{1,0:T(8,128)(2,1)S(1)}, bf16[256,256]{1,0:T(8,128)(2,1)}, u32[]{:S(2)}) copy-start(bf16[256,256]{1,0:T(8,128)(2,1)} %get-tuple-element.16) | copy-start | bytes 393220
  34.8 1.0 %copy-start = (bf16[256,256]{1,0:T(8,128)(2,1)S(1)}, bf16[256,256]{1,0:T(8,128)(2,1)}, u32[]{:S(2)}) copy-start(bf16[256,256]{1,0:T(8,128)(2,1)} %get-tuple-element.17) | copy-start | bytes 393220
  35.8 0.7 %copy-start.2 = (f32[2,128]{1,0:T(2,128)S(1)}, f32[2,128]{1,0:T(2,128)}, u32[]{:S(2)}) copy-start(f32[2,128]{1,0:T(2,128)} %get-tuple-element.19) | copy-start | bytes 3076

commit v2 on v1

--- a/solution.py
+++ b/solution.py
@@ -32,34 +32,50 @@
 
 def kernel(
     n_sp, n_tp,
-    q_ref, k_ref, v_ref, do_ref, g_ref, t_ref,
+    q_hbm, k_hbm, v_hbm, do_hbm, g_hbm, t_hbm,
     dq_ref, dk_ref, dv_ref, dt_ref, dg_ref,
-    k_raw, k_ext, v_ext, q_nxt, do_nxt, bias, bias_t, dk_acc, dv_acc,
+    q_ref, k_ref, do_ref, g_ref, t_ref, k_raw, k_ext, v_ext, q_nxt, do_nxt, bias, bias_t, dk_acc, dv_acc,
     st_out, st_in, red_src, red,
-    send_sem, recv_sem, red_send, red_recv,
+    load_sem, send_sem, recv_sem, red_send, red_recv,
 ):
     rows, width = q_ref.shape
     heads = width // HEAD_DIM
     half = rows // 2
     window = rows + half
-    entries = t_ref.shape[0]
+    entries = t_ref.shape[1]
     factor = HEAD_DIM ** (-0.5)
     sp, tp = lax.axis_index("sp"), lax.axis_index("tp")
     total = n_sp * n_tp
-    me = sp * n_tp + tp
     has_prev, has_next = sp > 0, sp < n_sp - 1
 
-    def place(offset):
-        other = lax.rem(me + offset, total)
-        return lax.div(other, n_tp), lax.rem(other, n_tp)
+    v_ref = v_ext.at[pl.ds(rows, rows)]
+    loads = [
+        pltpu.make_async_copy(src, dst, load_sem.at[i])
+        for i, (src, dst) in enumerate(
+            [(k_hbm, k_ref), (v_hbm, v_ref), (q_hbm, q_ref), (do_hbm, do_ref), (g_hbm, g_ref), (t_hbm, t_ref)]
+        )
+    ]
+    for load in loads:
+        load.start()
+
+    def everyone_else(action):
+        for other in range(n_tp - 1):
+            action(sp, lax.rem(tp + 1 + other, n_tp))
+
+        @pl.loop(1, n_sp)
+        def _(offset):
+            at = sp + offset
+            at = jnp.where(at >= n_sp, at - n_sp, at)
+            for other in range(n_tp):
+                action(at, other)
 
     barrier = pltpu.get_barrier_semaphore()
-
-    @pl.loop(1, total)
-    def _(offset):
-        pl.semaphore_signal(barrier, inc=1, device_id=place(offset), device_id_type=MESH)
-
+    everyone_else(
+        lambda at, core: pl.semaphore_signal(barrier, inc=1, device_id=(at, core), device_id_type=MESH)
+    )
     pl.semaphore_wait(barrier, total - 1)
+    for load in loads:
+        load.wait()
 
     def part(ref, index):
         return ref.at[pl.ds(index * half, half)]
@@ -85,15 +101,19 @@
     ]
     stats = [send(8 + i, st_out.at[i], st_in.at[i], prv) for i in range(2)]
 
-    @pl.when(has_next)
-    def _():
-        for copy in forward:
-            copy.start()
-
-    @pl.when(has_prev)
-    def _():
-        for copy in back:
-            copy.start()
+    def advance(done, started, gate=has_next):
+        if done:
+            @pl.when(has_next)
+            def _():
+                for copy in done:
+                    copy.wait_send()
+
+        @pl.when(gate)
+        def _():
+            for copy in started:
+                copy.start()
+
+    advance([], forward[:2])
 
     @pl.when(jnp.logical_not(has_prev))
     def _():
@@ -110,7 +130,7 @@
         + lax.broadcasted_iota(jnp.int32, (entries, rows), 1)
         == entries - 1
     ).astype(F32)
-    base = dot(t_ref[...], flip, (0, 0), lax.Precision.HIGHEST)
+    base = dot(t_ref[...], flip, (1, 0), lax.Precision.HIGHEST)
     for h in range(heads):
         far = base[h : h + 1, 0:1]
         near = pltpu.roll(
@@ -124,10 +144,10 @@
         bias_t[h, 0:half, :] = first[:, 0:half].T
         bias_t[h, half:, :] = near[:, 0:half].T
 
-    v_ext[rows:, :] = v_ref[...]
     for h in range(heads):
         k_ext[rows:, head[h]] = (unit_of(k_ref[:, head[h]])[0] * g1).astype(BF16)
 
+    advance(forward[:2], forward[2:])
     lane = lax.broadcasted_iota(jnp.int32, (half, HEAD_DIM), 1)
     window_col = lax.broadcasted_iota(jnp.int32, (1, window), 1)
     d_band = [None] * heads
@@ -142,6 +162,8 @@
                 k_ext[pair * half : (pair + 1) * half, head[h]] = (unit_of(block)[0] * g1).astype(BF16)
             forward[2 * (1 - pair) + 1].wait_recv()
 
+        if pair == 0:
+            advance(forward[2:], back, has_prev)
         own = slice(pair * half, (pair + 1) * half)
         span = slice(pair * half, pair * half + window)
         before = rows - pair * half
@@ -203,12 +225,12 @@
     slot = tp * n_sp + sp
     red[slot] = packed
 
-    @pl.loop(1, total)
-    def _(offset):
-        pltpu.make_async_remote_copy(
+    everyone_else(
+        lambda at, core: pltpu.make_async_remote_copy(
             src_ref=red_src, dst_ref=red.at[slot], send_sem=red_send, recv_sem=red_recv,
-            device_id=place(offset), device_id_type=MESH,
+            device_id=(at, core), device_id_type=MESH,
         ).start()
+    )
 
     @pl.when(has_next)
     def _():
@@ -249,21 +271,26 @@
         ],
         axis=0,
     )
-    dt_ref[...] = dot(flip, band, (1, 1), lax.Precision.HIGHEST)
+    dt_ref[...] = dot(band, flip, (1, 1), lax.Precision.HIGHEST)
     dg_ref[0:1, :] = everyone[2 * heads : 2 * heads + 1]
     dg_ref[1:2, :] = everyone[2 * heads + 1 : 2 * heads + 2] / g1
 
     pltpu.make_async_copy(peers, peers, red_send).wait()
-
-    @pl.when(has_next)
-    def _():
-        for copy in forward:
-            copy.wait_send()
 
     @pl.when(has_prev)
     def _():
         for copy in back + stats:
             copy.wait_send()
+
+
+def emit(*refs):
+    sem = refs[-1]
+    count = len(refs) // 2
+    copies = [pltpu.make_async_copy(refs[i], refs[count + i], sem.at[i]) for i in range(count)]
+    for copy in copies:
+        copy.start()
+    for copy in copies:
+        copy.wait()
 
 
 def solution(mesh):
@@ -277,16 +304,22 @@
         act = jax.ShapeDtypeStruct((rows, width), BF16)
         half = rows // 2
         vmem = pl.BlockSpec(memory_space=pltpu.VMEM)
-        return pl.pallas_call(
+        shapes = (
+            act, act, act,
+            jax.ShapeDtypeStruct(bias_table.shape[::-1], F32),
+            jax.ShapeDtypeStruct(gains.shape, F32),
+        )
+        parts = pl.pallas_call(
             functools.partial(kernel, n_sp, n_tp),
-            out_shape=(
-                act, act, act,
-                jax.ShapeDtypeStruct(bias_table.shape, F32),
-                jax.ShapeDtypeStruct(gains.shape, F32),
-            ),
-            in_specs=[vmem] * 6,
+            out_shape=shapes,
+            in_specs=[pl.BlockSpec(memory_space=pltpu.HBM)] * 6,
             out_specs=(vmem,) * 5,
             scratch_shapes=[
+                pltpu.VMEM((rows, width), BF16),
+                pltpu.VMEM((rows, width), BF16),
+                pltpu.VMEM((rows, width), BF16),
+                pltpu.VMEM(gains.shape, F32),
+                pltpu.VMEM(bias_table.shape[::-1], F32),
                 pltpu.VMEM((rows, width), BF16),
                 pltpu.VMEM((2 * rows, width), BF16),
                 pltpu.VMEM((2 * rows, width), BF16),
@@ -300,13 +333,28 @@
                 pltpu.VMEM((2, 8, half), F32),
                 pltpu.VMEM((8, HEAD_DIM), F32),
                 pltpu.VMEM((total, 8, HEAD_DIM), F32),
+                pltpu.SemaphoreType.DMA((6,)),
                 pltpu.SemaphoreType.DMA((10,)),
                 pltpu.SemaphoreType.DMA((10,)),
                 pltpu.SemaphoreType.DMA,
                 pltpu.SemaphoreType.DMA,
             ],
-            compiler_params=pltpu.CompilerParams(collective_id=0, has_side_effects=True),
-        )(queries, keys, values, d_out, gains, bias_table)
+            compiler_params=pltpu.CompilerParams(
+                collective_id=0, has_side_effects=True, vmem_limit_bytes=16 * 1024 * 1024
+            ),
+        )(*(
+            pltpu.with_memory_space_constraint(x, pltpu.HBM)
+            for x in (queries, keys, values, d_out, gains, bias_table.T)
+        ))
+        d_q, d_k, d_v, d_table, d_gains = pl.pallas_call(
+            emit,
+            out_shape=shapes,
+            in_specs=[vmem] * 5,
+            out_specs=(pl.BlockSpec(memory_space=pltpu.HBM),) * 5,
+            scratch_shapes=[pltpu.SemaphoreType.DMA((5,))],
+            compiler_params=pltpu.CompilerParams(vmem_limit_bytes=8 * 1024 * 1024),
+        )(*parts)
+        return d_q, d_k, d_v, d_table.T, d_gains
 
     in_specs = (P("sp", "tp"), P("sp", "tp"), P("sp", "tp"), P(), P(None, "tp"), P("sp", "tp"))
     out_specs = (P("sp", "tp"), P("sp", "tp"), P("sp", "tp"), P(None, "tp"), P())

time: 37.3 us -> 26.1 us (0.70)
  local copies, waits for them, and re-layouts: 6.78 us -> 0 us
  Pallas kernels: 29.6 us -> 25.3 us
    unnamed x11 -> x0, local copies, waits for them, and re-layouts: 5.23 us -> none
    pallas_call x1 -> x2, Pallas kernels: 29.6 us -> 25.3 us  [the longest x1 24.5 us: local(): pl.pallas_call(functools.partial(kernel, n_sp, n_tp), out_shape=shapes, i...]
    pallas_call x1 -> x0, local copies, waits for them, and re-layouts: 1.55 us -> none  [local(): pl.pallas_call(functools.partial(kernel, n_sp, n_tp), out_shape=(act, act...]
where the time goes in v2:
time: 26.1 us; the launch traced here: 25.9 us
  Pallas kernels  25.3 us (97%)
  between operations  0.64 us (2%)
    pallas_call x1, Pallas kernels, local(): pl.pallas_call(functools.partial(kernel, n_sp, n_tp), out_shape=shapes, i...  24.5 us
    pallas_call x1, Pallas kernels, local(): pl.pallas_call(emit, out_shape=shapes, in_specs=[vmem] * 5, out_specs=(pl...  0.79 us

profile of v2, /device:TPU:0, one launch (start us, length us, event | category | flops | bytes accessed | tf_op | source)
XLA Modules:
  0.0 25.9 jit_solution(12512055629742691691)
XLA Ops:
  0.6 24.5 %shard_map.101 = (bf16[256,256]{1,0:T(8,128)(2,1)S(1)}, bf16[256,256]{1,0:T(8,128)(2,1)S(1)}, bf16[256,256]{1,0:T(8,128)(2,1)S(1)}, f32[2,192]{1,0:T(2,128)S(1)}, f32[2,128]{1,0:T(2,128)S(1)}) custom-call(bf16[256,256]{1,0:T(8,128)(2,1)} %q_hbm.1, bf16[256,256]{1,0:T(8,128)(2,1)} %k_hbm.1, bf16[256,256]{1,0:T(8,128)(2,1)} %v_hbm.1, bf16[256,256]{1,0:T(8,128)(2,1)} %do_hbm.1, ...), custom_call_target="tpu_custom_call" | custom-call | tf_op jit(solution)/shard_map/pallas_call | solution.py:312
  25.1 0.8 %shard_map.102 = (bf16[256,256]{1,0:T(8,128)(2,1)}, bf16[256,256]{1,0:T(8,128)(2,1)}, bf16[256,256]{1,0:T(8,128)(2,1)}, f32[2,192]{1,0:T(2,128)}, f32[2,128]{1,0:T(2,128)}) custom-call(bf16[256,256]{1,0:T(8,128)(2,1)S(1)} %get-tuple-element.15.refs_0_, bf16[256,256]{1,0:T(8,128)(2,1)S(1)} %get-tuple-element.16.refs_1_, ...), custom_call_target="tpu_custom_call" | custom-call | tf_op jit(solution)/shard_map/pallas_call | solution.py:349

commit v3 on v2

--- a/solution.py
+++ b/solution.py
@@ -35,8 +35,8 @@
     q_hbm, k_hbm, v_hbm, do_hbm, g_hbm, t_hbm,
     dq_ref, dk_ref, dv_ref, dt_ref, dg_ref,
     q_ref, k_ref, do_ref, g_ref, t_ref, k_raw, k_ext, v_ext, q_nxt, do_nxt, bias, bias_t, dk_acc, dv_acc,
-    st_out, st_in, red_src, red,
-    load_sem, send_sem, recv_sem, red_send, red_recv,
+    st_out, st_in, one_src, one, two_src, two,
+    load_sem, send_sem, recv_sem, red_sem,
 ):
     rows, width = q_ref.shape
     heads = width // HEAD_DIM
@@ -45,7 +45,6 @@
     entries = t_ref.shape[1]
     factor = HEAD_DIM ** (-0.5)
     sp, tp = lax.axis_index("sp"), lax.axis_index("tp")
-    total = n_sp * n_tp
     has_prev, has_next = sp > 0, sp < n_sp - 1
 
     v_ref = v_ext.at[pl.ds(rows, rows)]
@@ -58,22 +57,32 @@
     for load in loads:
         load.start()
 
-    def everyone_else(action):
-        for other in range(n_tp - 1):
-            action(sp, lax.rem(tp + 1 + other, n_tp))
-
-        @pl.loop(1, n_sp)
+    side, team = lax.rem(sp, 2), lax.div(sp, 2)
+    teams = n_sp // 2
+
+    def team_mates(action):
+        for other in range(1, n_tp):
+            action(sp, lax.rem(tp + other, n_tp))
+        for other in range(n_tp):
+            action(2 * team + 1 - side, lax.rem(tp + other, n_tp))
+
+    def other_teams(action):
+        @pl.loop(1, teams)
         def _(offset):
-            at = sp + offset
-            at = jnp.where(at >= n_sp, at - n_sp, at)
-            for other in range(n_tp):
-                action(at, other)
+            at = team + offset
+            at = jnp.where(at >= teams, at - teams, at)
+            action(2 * at + side, tp)
+
+    def greet(at, core):
+        pl.semaphore_signal(barrier, inc=1, device_id=(at, core), device_id_type=MESH)
 
     barrier = pltpu.get_barrier_semaphore()
-    everyone_else(
-        lambda at, core: pl.semaphore_signal(barrier, inc=1, device_id=(at, core), device_id_type=MESH)
-    )
-    pl.semaphore_wait(barrier, total - 1)
+    greet(lax.rem(sp + 1, n_sp), tp)
+    greet(lax.rem(sp + n_sp - 1, n_sp), tp)
+    team_mates(greet)
+    other_teams(greet)
+    mates = 2 * n_tp - 1
+    pl.semaphore_wait(barrier, 2 + mates + teams - 1)
     for load in loads:
         load.wait()
 
@@ -163,7 +172,7 @@
             forward[2 * (1 - pair) + 1].wait_recv()
 
         if pair == 0:
-            advance(forward[2:], back, has_prev)
+            advance(forward[2:], back[:2], has_prev)
         own = slice(pair * half, (pair + 1) * half)
         span = slice(pair * half, pair * half + window)
         before = rows - pair * half
@@ -221,13 +230,27 @@
     lines += [gain_q, gain_k]
     lines += [jnp.zeros((8 - len(lines), HEAD_DIM), F32)]
     packed = jnp.concatenate(lines, axis=0)
-    red_src[...] = packed
-    slot = tp * n_sp + sp
-    red[slot] = packed
-
-    everyone_else(
+    one_src[...] = packed
+    place = side * n_tp + tp
+    one[place] = packed
+    team_mates(
         lambda at, core: pltpu.make_async_remote_copy(
-            src_ref=red_src, dst_ref=red.at[slot], send_sem=red_send, recv_sem=red_recv,
+            src_ref=one_src, dst_ref=one.at[place], send_sem=red_sem.at[0], recv_sem=red_sem.at[1],
+            device_id=(at, core), device_id_type=MESH,
+        ).start()
+    )
+    advance([], back[2:], has_prev)
+    near_peers = one.at[pl.ds(0, mates)]
+    pltpu.make_async_copy(near_peers, near_peers, red_sem.at[1]).wait()
+    whole = jnp.sum(one[...], axis=0)
+    same = one[tp] + one[n_tp + tp]
+    line = lax.broadcasted_iota(jnp.int32, whole.shape, 0)
+    joined = jnp.where(line < 2 * heads, same, whole)
+    two_src[...] = joined
+    two[team] = joined
+    other_teams(
+        lambda at, core: pltpu.make_async_remote_copy(
+            src_ref=two_src, dst_ref=two.at[team], send_sem=red_sem.at[2], recv_sem=red_sem.at[3],
             device_id=(at, core), device_id_type=MESH,
         ).start()
     )
@@ -260,10 +283,9 @@
         out = rms * (grad - unit * jnp.mean(grad * unit, axis=-1, keepdims=True))
         dk_ref[:, head[h]] = out.astype(BF16)
 
-    peers = red.at[pl.ds(0, total - 1)]
-    pltpu.make_async_copy(peers, peers, red_recv).wait()
-    everyone = jnp.sum(red[...], axis=0)
-    mine = jnp.sum(red[pl.ds(tp * n_sp, n_sp)], axis=0)
+    far_peers = two.at[pl.ds(0, teams - 1)]
+    pltpu.make_async_copy(far_peers, far_peers, red_sem.at[3]).wait()
+    mine = jnp.sum(two[...], axis=0)
     band = jnp.concatenate(
         [
             jnp.concatenate([mine[2 * h : 2 * h + 1], mine[2 * h + 1 : 2 * h + 2]], axis=1)
@@ -272,10 +294,11 @@
         axis=0,
     )
     dt_ref[...] = dot(band, flip, (1, 1), lax.Precision.HIGHEST)
-    dg_ref[0:1, :] = everyone[2 * heads : 2 * heads + 1]
-    dg_ref[1:2, :] = everyone[2 * heads + 1 : 2 * heads + 2] / g1
-
-    pltpu.make_async_copy(peers, peers, red_send).wait()
+    dg_ref[0:1, :] = mine[2 * heads : 2 * heads + 1]
+    dg_ref[1:2, :] = mine[2 * heads + 1 : 2 * heads + 2] / g1
+
+    pltpu.make_async_copy(near_peers, near_peers, red_sem.at[0]).wait()
+    pltpu.make_async_copy(far_peers, far_peers, red_sem.at[2]).wait()
 
     @pl.when(has_prev)
     def _():
@@ -299,8 +322,7 @@
     def local(queries, keys, values, gains, bias_table, d_out):
         rows, width = queries.shape
         heads = width // HEAD_DIM
-        assert rows == LEFT * SEG and 2 * heads + 2 <= 8
-        total = n_sp * n_tp
+        assert n_sp % 2 == 0 and n_sp > 2 and rows == LEFT * SEG and 2 * heads + 2 <= 8
         act = jax.ShapeDtypeStruct((rows, width), BF16)
         half = rows // 2
         vmem = pl.BlockSpec(memory_space=pltpu.VMEM)
@@ -332,12 +354,13 @@
                 pltpu.VMEM((2, 8, half), F32),
                 pltpu.VMEM((2, 8, half), F32),
                 pltpu.VMEM((8, HEAD_DIM), F32),
-                pltpu.VMEM((total, 8, HEAD_DIM), F32),
+                pltpu.VMEM((2 * n_tp, 8, HEAD_DIM), F32),
+                pltpu.VMEM((8, HEAD_DIM), F32),
+                pltpu.VMEM((n_sp // 2, 8, HEAD_DIM), F32),
                 pltpu.SemaphoreType.DMA((6,)),
                 pltpu.SemaphoreType.DMA((10,)),
                 pltpu.SemaphoreType.DMA((10,)),
-                pltpu.SemaphoreType.DMA,
-                pltpu.SemaphoreType.DMA,
+                pltpu.SemaphoreType.DMA((4,)),
             ],
             compiler_params=pltpu.CompilerParams(
                 collective_id=0, has_side_effects=True, vmem_limit_bytes=16 * 1024 * 1024

time: 26.1 us -> 24.5 us (0.939)
  Pallas kernels: 25.3 us -> 23.7 us
    pallas_call x1, Pallas kernels: 24.5 us -> 22.9 us  [local(): pl.pallas_call(functools.partial(kernel, n_sp, n_tp), out_shape=shapes, i...]
where the time goes in v3:
time: 24.5 us; the launch traced here: 24.3 us
  Pallas kernels  23.7 us (97%)
  between operations  0.64 us (3%)
    pallas_call x1, Pallas kernels, local(): pl.pallas_call(functools.partial(kernel, n_sp, n_tp), out_shape=shapes, i...  22.9 us
    pallas_call x1, Pallas kernels, local(): pl.pallas_call(emit, out_shape=shapes, in_specs=[vmem] * 5, out_specs=(pl...  0.79 us

profile of v3, /device:TPU:0, one launch (start us, length us, event | category | flops | bytes accessed | tf_op | source)
XLA Modules:
  0.0 24.3 jit_solution(17671308492289698822)
XLA Ops:
  0.6 22.9 %shard_map.101 = (bf16[256,256]{1,0:T(8,128)(2,1)S(1)}, bf16[256,256]{1,0:T(8,128)(2,1)S(1)}, bf16[256,256]{1,0:T(8,128)(2,1)S(1)}, f32[2,192]{1,0:T(2,128)S(1)}, f32[2,128]{1,0:T(2,128)S(1)}) custom-call(bf16[256,256]{1,0:T(8,128)(2,1)} %q_hbm.1, bf16[256,256]{1,0:T(8,128)(2,1)} %k_hbm.1, bf16[256,256]{1,0:T(8,128)(2,1)} %v_hbm.1, bf16[256,256]{1,0:T(8,128)(2,1)} %do_hbm.1, ...), custom_call_target="tpu_custom_call" | custom-call | tf_op jit(solution)/shard_map/pallas_call | solution.py:334
  23.5 0.8 %shard_map.102 = (bf16[256,256]{1,0:T(8,128)(2,1)}, bf16[256,256]{1,0:T(8,128)(2,1)}, bf16[256,256]{1,0:T(8,128)(2,1)}, f32[2,192]{1,0:T(2,128)}, f32[2,128]{1,0:T(2,128)}) custom-call(bf16[256,256]{1,0:T(8,128)(2,1)S(1)} %get-tuple-element.15.refs_0_, bf16[256,256]{1,0:T(8,128)(2,1)S(1)} %get-tuple-element.16.refs_1_, ...), custom_call_target="tpu_custom_call" | custom-call | tf_op jit(solution)/shard_map/pallas_call | solution.py:372
